TPU v7x, 256 devices: a whole 4x4x8 slice. The times are simulated.
256 devices in a mesh: ep: 16 (over y, x), tp: 16 (over z, core).
Axes of the slice: x: 4, y: 4, z: 8, core: 2. Of those that a mesh axis runs over, the one named last changes fastest.
Arguments:
- mix_tokens: bfloat16 [32768, 2048], P(('ep', 'tp')), may hold values from -6 to 6
- mix_gain: bfloat16 [2048], replicated, may hold values from 0.099609375 to 1.8984375
- gate_proj: bfloat16 [2048, 1024], P(None, 'tp'), may hold values from -0.125 to 0.125
- conv_proj: bfloat16 [2048, 1024], P(None, 'tp'), may hold values from -0.125 to 0.125
- value_proj: bfloat16 [2048, 1024], P(None, 'tp'), may hold values from -0.125 to 0.125
- conv_taps: bfloat16 [3, 1024], P(None, 'tp'), may hold values from -3 to 3
- out_proj: bfloat16 [1024, 2048], P('tp'), may hold values from -0.1875 to 0.1875
- moe_tokens: bfloat16 [16384, 2048], P(('ep', 'tp')), may hold values from -6 to 6
- moe_gain: bfloat16 [2048], replicated, may hold values from 0.099609375 to 1.8984375
- expert_ids: int32 [16384, 2], P(('ep', 'tp')), may hold values from 0 to 15, all different within a row; in each aligned block of 64 rows (0 to 63, 64 to 127, ...) at most 9 rows name the same one
- expert_scores: float32 [16384, 2], P(('ep', 'tp')), may hold values from -6 to 6
- expert_gate: bfloat16 [16, 2048, 4096], P('ep', None, 'tp'), may hold values from -0.125 to 0.125
- expert_up: bfloat16 [16, 2048, 4096], P('ep', None, 'tp'), may hold values from -0.125 to 0.125
- expert_down: bfloat16 [16, 4096, 2048], P('ep', 'tp'), may hold values from -0.09375 to 0.09375
Outputs:
- mix_out: bfloat16 [32768, 2048], P(('ep', 'tp'))
- moe_out: bfloat16 [16384, 2048], P(('ep', 'tp'))
Inputs may be any that keep to these rules, and one draw needn't show every extreme that they name: `expert_ids`: each row names 2 different experts; among the rows of one device no expert is named more than 9 times.
All inputs are finite; a program needn't handle non-finite values.
Results may differ from a plain program's by a relative error of at most 0.018.
Values may be sent and summed in bfloat16 or wider, within the bound.
A program may use at most 128 MiB of HBM per device.

v0:
```python
import jax
import jax.numpy as jnp
from jax import lax
from jax.sharding import PartitionSpec as P

norm_eps = 1e-06


def from_behind(value, axis, steps):
    count = lax.axis_size(axis)
    leading, last = (max(0, -steps), min(count, count - steps))
    return lax.ppermute(value, axis, [(source, source + steps) for source in range(leading, last)])


def scaled_norm(row_data, gain_vec):
    values = row_data.astype(jnp.float32)
    inverse = lax.rsqrt(jnp.mean(values * values, axis=1, keepdims=True) + norm_eps)
    return (values * inverse * gain_vec.astype(jnp.float32)).astype(jnp.bfloat16)


def shards(
    mix_tokens,
    mix_gain,
    gate_proj,
    conv_proj,
    value_proj,
    conv_taps,
    out_proj,
    moe_tokens,
    moe_gain,
    expert_ids,
    expert_scores,
    expert_gate,
    expert_up,
    expert_down,
):
    normed = scaled_norm(mix_tokens, mix_gain)
    w_joint = jnp.concatenate([gate_proj, conv_proj, value_proj], axis=1)
    combined = jnp.dot(
        lax.all_gather(normed, "tp", axis=0, tiled=True),
        w_joint,
        preferred_element_type=jnp.float32,
    ).astype(jnp.bfloat16)
    channels = gate_proj.shape[1]
    out_gate = combined[:, :channels]
    in_gate = combined[:, channels : 2 * channels]
    values = combined[:, 2 * channels :]
    signal = (in_gate.astype(jnp.float32) * values.astype(jnp.float32)).astype(jnp.bfloat16)
    tap_count = conv_taps.shape[0]
    before = from_behind(signal[signal.shape[0] - (tap_count - 1) :], "ep", 1)
    extended = jnp.concatenate([before, signal], axis=0)
    length = signal.shape[0]
    tap_values = conv_taps.astype(jnp.float32)
    convolved = jnp.zeros((length, channels), jnp.float32)
    for offset in range(tap_count):
        convolved = (
            convolved + extended[offset : offset + length].astype(jnp.float32) * tap_values[offset]
        )
    carried = (out_gate.astype(jnp.float32) * convolved).astype(jnp.bfloat16)
    token_major = lax.all_to_all(carried, "tp", split_axis=0, concat_axis=1, tiled=True)
    mix_out = jnp.dot(
        token_major,
        lax.all_gather(out_proj, "tp", axis=0, tiled=True),
        preferred_element_type=jnp.float32,
    ).astype(jnp.bfloat16)
    moe_normed = scaled_norm(moe_tokens, moe_gain)
    experts = expert_gate.shape[0] * lax.axis_size("ep")
    row_count, top_count = expert_ids.shape
    capacity = top_count * row_count // experts + max(1, top_count * row_count // (8 * experts))
    width_model = moe_tokens.shape[1]
    flat_ids = expert_ids.reshape(-1)
    onehot = (flat_ids[:, None] == jnp.arange(experts, dtype=jnp.int32)[None, :]).astype(jnp.int32)
    slot_rank = jnp.sum((jnp.cumsum(onehot, axis=0) - onehot) * onehot, axis=1)
    slot_index = flat_ids * capacity + slot_rank
    slot_match = slot_index[:, None] == jnp.arange(experts * capacity, dtype=jnp.int32)[None, :]
    dispatch_map = jnp.any(
        slot_match.reshape(row_count, top_count, experts * capacity), axis=1
    ).astype(jnp.bfloat16)
    outgoing = lax.dot_general(
        dispatch_map, moe_normed, (((0,), (0,)), ((), ())), preferred_element_type=jnp.float32
    ).astype(jnp.bfloat16)
    arrived = lax.all_to_all(
        outgoing.reshape(experts, capacity, width_model),
        "ep",
        split_axis=0,
        concat_axis=0,
        tiled=True,
    )
    arrived_rows = arrived.reshape(-1, width_model)
    w_gate = expert_gate[0]
    w_up = expert_up[0]
    w_down = expert_down[0]
    portion = lax.all_gather(arrived_rows, "tp", axis=0, tiled=True)
    gate_value = jnp.dot(portion, w_gate, preferred_element_type=jnp.float32)
    up_value = jnp.dot(portion, w_up, preferred_element_type=jnp.float32)
    hidden = (jax.nn.silu(gate_value) * up_value).astype(jnp.bfloat16)
    summed = lax.psum_scatter(
        jnp.dot(hidden, w_down, preferred_element_type=jnp.float32).astype(jnp.bfloat16),
        "tp",
        scatter_dimension=0,
        tiled=True,
    )
    returned = lax.all_to_all(
        summed.reshape(experts, capacity, width_model),
        "ep",
        split_axis=0,
        concat_axis=0,
        tiled=True,
    )
    flat_back = returned.reshape(experts * capacity, width_model)
    picked = flat_back[slot_index].reshape(row_count, top_count, width_model)
    route_weight = jax.nn.softmax(expert_scores, axis=1)
    moe_out = jnp.sum(route_weight[:, :, None] * picked.astype(jnp.float32), axis=1).astype(
        jnp.bfloat16
    )
    return (mix_out, moe_out)


def solution(mesh):
    in_specs = (
        P(("ep", "tp"), None),
        P(),
        P(None, "tp"),
        P(None, "tp"),
        P(None, "tp"),
        P(None, "tp"),
        P("tp", None),
        P(("ep", "tp"), None),
        P(),
        P(("ep", "tp"), None),
        P(("ep", "tp"), None),
        P("ep", None, "tp"),
        P("ep", None, "tp"),
        P("ep", "tp", None),
    )
    out_specs = (P(("ep", "tp"), None), P(("ep", "tp"), None))
    return jax.shard_map(shards, mesh=mesh, in_specs=in_specs, out_specs=out_specs, check_vma=False)
```

profile of v0, /device:TPU:2, one launch (start us, length us, event | category | flops | bytes accessed | tf_op | source)
XLA Modules:
  0.0 290.8 jit_solution(8549273080741177627)
XLA Ops:
  7.2 0.8 copy.25
  9.0 0.7 convert_element_type.89
  9.7 1.1 fusion.15
  10.8 1.3 convolution_convert_fusion.2
  12.4 23.1 %all_to_all.29 = bf16[16,9,2048]{2,1,0:T(8,128)(2,1)S(1)} all-to-all(bf16[16,9,2048]{2,1,0:T(8,128)(2,1)S(1)} %reshape.87), channel_id=1, replica_groups=mesh['ep'=16,'tp'=16] {'ep'}, dimensions={0} | all-to-all | bytes 1179648 | tf_op jit(solution)/shard_map/all_to_all | solution.py:82
  35.5 1.1 reshape.88
  36.8 1.0 fusion.4
  37.9 59.6 %all-gather.8.cloned.1.call-done = bf16[2304,2048]{1,0:T(8,128)(2,1)} async-done(((bf16[144,2048]{1,0:T(8,128)(2,1)}), bf16[2304,2048]{1,0:T(8,128)(2,1)}) %all-gather.8.cloned.1.call-update) | async-done | bytes 9437200 | tf_op jit(solution)/shard_map/all_gather | solution.py:93
  97.5 7.7 %fusion.8 = f32[2304,256]{1,0:T(8,128)} fusion(bf16[2304,2048]{1,0:T(8,128)(2,1)} %all-gather.8.cloned.1.call-done, bf16[1,2048,256]{2,1,0:T(8,128)(2,1)S(1)} %copy-done.5), kind=kOutput, calls=%fused_computation.15 | convolution fusion | flops 2415919104 | bytes 12845056 | tf_op jit(solution)/shard_map/dot_general | solution.py:94
  105.2 14.9 %convolution_convert_fusion = bf16[2304,2048]{1,0:T(8,128)(2,1)} fusion(bf16[2304,2048]{1,0:T(8,128)(2,1)} %all-gather.8.cloned.1.call-done, f32[2304,256]{1,0:T(8,128)} %fusion.8, bf16[1,256,2048]{2,1,0:T(8,128)(2,1)S(1)} %copy-done, bf16[1,2048,256]{2,1,0:T(8,128)(2,1)} %param.26), kind=kOutput, calls=%fused_computation.1 | convolution fusion | flops 4840095744 | bytes 23330816 | tf_op jit(solution)/shard_map/dot_general | solution.py:98
  120.8 33.5 %all-gather.4.cloned.1.call-done = bf16[2048,2048]{1,0:T(8,128)(2,1)} async-done(((bf16[128,2048]{1,0:T(8,128)(2,1)}), bf16[2048,2048]{1,0:T(8,128)(2,1)}) %all-gather.4.cloned.1.call-update) | async-done | bytes 8388624 | tf_op jit(solution)/shard_map/all_gather | solution.py:40
  154.3 6.3 %convolution_convert_fusion.1 = bf16[2048,192]{0,1:T(8,128)(2,1)S(1)} fusion(bf16[2048,2048]{1,0:T(8,128)(2,1)} %all-gather.4.cloned.1.call-done, bf16[2048,64]{0,1:T(8,128)(2,1)S(1)} %copy-done.6, bf16[2048,64]{0,1:T(8,128)(2,1)S(1)} %copy-done.7, bf16[2048,64]{0,1:T(8,128)(2,1)S(1)} %copy-done.8), kind=kOutput, calls=%fused_computation.4 | convolution fusion | flops 1613365248 | bytes 9961472 | tf_op jit(solution)/shard_map/dot_general | solution.py:39
  160.8 3.4 %collective-permute-start = (bf16[2,64]{0,1:T(8,128)(2,1)S(1)}, bf16[2,64]{0,1:T(8,128)(2,1)S(1)}, u32[]{:S(2)}, u32[]{:S(2)}) collective-permute-start(bf16[2,64]{0,1:T(8,128)(2,1)S(1)} %slice.41), channel_id=1, source_target_pairs={{0,16},{16,32},{32,48},{48,64},{64,80},{80,96},{96,112},{112,128},... | collective-permute-start | bytes 776 | tf_op jit(solution)/shard_map/ppermute | solution.py:12
  164.2 2.2 collective-permute-done
  166.4 1.0 copy_bitcast_fusion
  167.4 4.4 %all-to-all-start = ((bf16[16,128,64]{1,2,0:T(8,128)(2,1)}), bf16[16,128,64]{1,2,0:T(8,128)(2,1)S(1)}, u32[]{:S(2)}, u32[]{:S(2)}) async-start(bf16[16,128,64]{1,2,0:T(8,128)(2,1)} %copy_bitcast_fusion), calls=%async_computation | async-start | bytes 524288 | tf_op jit(solution)/shard_map/all_to_all | solution.py:60
  172.0 61.9 %reduce-scatter.2.cloned.1.call-done = bf16[144,2048]{1,0:T(8,128)(2,1)} async-done(((bf16[2304,2048]{1,0:T(8,128)(2,1)}), bf16[144,2048]{1,0:T(8,128)(2,1)}) %reduce-scatter.2.cloned.1.call-update) | async-done | bytes 589840 | tf_op jit(solution)/shard_map/reduce_scatter | solution.py:97
  233.9 2.3 reshape.89
  236.2 7.4 %all-to-all-start.2 = ((bf16[16,9,2048]{2,1,0:T(8,128)(2,1)}), bf16[16,9,2048]{2,1,0:T(8,128)(2,1)S(1)}, u32[]{:S(2)}, u32[]{:S(2)}) async-start(bf16[16,9,2048]{2,1,0:T(8,128)(2,1)} %reshape.89), calls=%async_computation.3 | async-start | bytes 2097152 | tf_op jit(solution)/shard_map/all_to_all | solution.py:103
  243.7 32.7 %all-gather.6.cloned.1.call-done = bf16[1024,2048]{1,0:T(8,128)(2,1)} async-done(((bf16[64,2048]{1,0:T(8,128)(2,1)}), bf16[1024,2048]{1,0:T(8,128)(2,1)}) %all-gather.6.cloned.1.call-update) | async-done | bytes 4194320 | tf_op jit(solution)/shard_map/all_gather | solution.py:63
  276.4 3.7 %convolution_convert_fusion.3 = bf16[128,2048]{1,0:T(8,128)(2,1)} fusion(bf16[128,1024]{0,1:T(8,128)(2,1)S(1)} %bitcast.36, bf16[1024,2048]{1,0:T(8,128)(2,1)} %all-gather.6.cloned.1.call-done), kind=kOutput, calls=%fused_computation.6 | convolution fusion | flops 537133056 | bytes 4980736 | tf_op jit(solution)/shard_map/dot_general | solution.py:61
  280.4 0.9 gather_fusion
  281.3 0.7 reshape.91
  282.0 2.2 multiply_reduce_fusion
  (53 shorter events, 2.9 us)
Async XLA Ops:
  7.2 98.0 %copy-start = (bf16[1,256,2048]{2,1,0:T(8,128)(2,1)S(1)}, bf16[1,256,2048]{2,1,0:T(8,128)(2,1)}, u32[]{:S(2)}) copy-start(bf16[1,256,2048]{2,1,0:T(8,128)(2,1)} %param.27) | copy-start | bytes 3145732
  7.2 90.3 %all-gather.8.cloned.1.call-start = ((), (), s32[]{:S(2)}) async-start(), calls=%async_computation.6 | async-start | bytes 10027008 | tf_op jit(solution)/shard_map/all_gather | solution.py:93
  12.4 24.2 %copy-start.3 = (bf16[2048]{0:T(1024)(128)(2,1)S(1)}, bf16[2048]{0:T(1024)(128)(2,1)}, u32[]{:S(2)}) copy-start(bf16[2048]{0:T(1024)(128)(2,1)} %param.15) | copy-start | bytes 12292
  35.5 1.2 copy-start.1
  36.5 61.0 %copy-start.5 = (bf16[1,2048,256]{2,1,0:T(8,128)(2,1)S(1)}, bf16[1,2048,256]{2,1,0:T(8,128)(2,1)}, u32[]{:S(2)}) copy-start(bf16[1,2048,256]{2,1,0:T(8,128)(2,1)} %param.25) | copy-start | bytes 3145732
  36.6 117.7 %all-gather.4.cloned.1.call-start = ((), (), s32[]{:S(2)}) async-start(), calls=%async_computation.4 | async-start | bytes 8912896 | tf_op jit(solution)/shard_map/all_gather | solution.py:40
  37.9 196.0 %reduce-scatter.2.cloned.1.call-start = ((), (), s32[]{:S(2)}) async-start(), calls=%async_computation.7 | async-start | bytes 10027008 | tf_op jit(solution)/shard_map/reduce_scatter | solution.py:97
  120.1 0.7 copy-start.4
  120.1 34.2 %copy-start.6 = (bf16[2048,64]{0,1:T(8,128)(2,1)S(1)}, bf16[2048,64]{0,1:T(8,128)(2,1)}, u32[]{:S(2)}) copy-start(bf16[2048,64]{0,1:T(8,128)(2,1)} %param.18) | copy-start | bytes 786436
  120.1 34.2 %copy-start.7 = (bf16[2048,64]{0,1:T(8,128)(2,1)S(1)}, bf16[2048,64]{0,1:T(8,128)(2,1)}, u32[]{:S(2)}) copy-start(bf16[2048,64]{0,1:T(8,128)(2,1)} %param.17) | copy-start | bytes 786436
  120.1 34.2 %copy-start.8 = (bf16[2048,64]{0,1:T(8,128)(2,1)S(1)}, bf16[2048,64]{0,1:T(8,128)(2,1)}, u32[]{:S(2)}) copy-start(bf16[2048,64]{0,1:T(8,128)(2,1)} %param.16) | copy-start | bytes 786436
  120.2 156.2 %all-gather.6.cloned.1.call-start = ((), (), s32[]{:S(2)}) async-start(), calls=%async_computation.5 | async-start | bytes 4456448 | tf_op jit(solution)/shard_map/all_gather | solution.py:63
  120.8 51.1 %copy-start.2 = (f32[64,2]{0,1:T(2,128)S(1)}, f32[64,2]{0,1:T(2,128)}, u32[]{:S(2)}) copy-start(f32[64,2]{0,1:T(2,128)} %param.24) | copy-start | bytes 1540
  160.8 5.6 %collective-permute-start = (bf16[2,64]{0,1:T(8,128)(2,1)S(1)}, bf16[2,64]{0,1:T(8,128)(2,1)S(1)}, u32[]{:S(2)}, u32[]{:S(2)}) collective-permute-start(bf16[2,64]{0,1:T(8,128)(2,1)S(1)} %slice.41), channel_id=1, source_target_pairs={{0,16},{16,32},{32,48},{48,64},{64,80},{80,96},{96,112},{112,128},... | collective-permute-start | bytes 776 | tf_op jit(solution)/shard_map/ppermute | solution.py:12
  167.4 68.7 %all-to-all-start = ((bf16[16,128,64]{1,2,0:T(8,128)(2,1)}), bf16[16,128,64]{1,2,0:T(8,128)(2,1)S(1)}, u32[]{:S(2)}, u32[]{:S(2)}) async-start(bf16[16,128,64]{1,2,0:T(8,128)(2,1)} %copy_bitcast_fusion), calls=%async_computation | async-start | bytes 524288 | tf_op jit(solution)/shard_map/all_to_all | solution.py:60
  236.2 44.0 %all-to-all-start.2 = ((bf16[16,9,2048]{2,1,0:T(8,128)(2,1)}), bf16[16,9,2048]{2,1,0:T(8,128)(2,1)S(1)}, u32[]{:S(2)}, u32[]{:S(2)}) async-start(bf16[16,9,2048]{2,1,0:T(8,128)(2,1)} %reshape.89), calls=%async_computation.3 | async-start | bytes 2097152 | tf_op jit(solution)/shard_map/all_to_all | solution.py:103
Sparse Core Ops, SparseCore 0:
  36.7 60.7 all-gather.7
  99.9 54.3 all-gather.3
  156.9 76.9 reduce-scatter.1
  235.6 40.8 all-gather.5
where the time goes:
time: 293 us; the launch traced here: 291 us
  waiting for transfers between devices  190 us (65%)
  matrix products  34 us (12%)
  blocking collectives  23.1 us (8%)
  starting transfers between devices  15.3 us (5%)
  between operations  14 us (5%)
  local copies, waits for them, and re-layouts  7.03 us (2%)
  other arithmetic  6.89 us (2%)
    reduce_scatter x1, waiting for transfers between devices, shards(): lax.psum_scatter(jnp.dot(hidden, w_down, preferred_element_type=jnp.float...  61.9 us
    all_gather x1, waiting for transfers between devices, shards(): portion = lax.all_gather(arrived_rows, 'tp', axis=0, tiled=True)  59.6 us
    all_gather x1, waiting for transfers between devices, shards(): lax.all_gather(normed, 'tp', axis=0, tiled=True)  33.5 us
    all_gather x1, waiting for transfers between devices, shards(): lax.all_gather(out_proj, 'tp', axis=0, tiled=True)  32.7 us
    all_to_all x1, blocking collectives, shards(): lax.all_to_all(outgoing.reshape(experts, capacity, width_model), 'ep', sp...  23.1 us
    dot_general x1, matrix products, shards(): jnp.dot(hidden, w_down, preferred_element_type=jnp.float32)  14.9 us
    dot_general x1, matrix products, shards(): gate_value = jnp.dot(portion, w_gate, preferred_element_type=jnp.float32)  7.72 us
    all_to_all x1, starting transfers between devices, shards(): lax.all_to_all(summed.reshape(experts, capacity, width_model), 'ep', spli...  7.43 us
  transfers between devices with their start and end apart: 7, of which 5 were waited for; matrix products, arithmetic and copies ran while one was open for 13% of the time, Pallas kernels for 0%

commit v1 on v0

v1 whole, which is shorter than its diff:
```python
import jax
import jax.numpy as jnp
from jax import lax
from jax.experimental import pallas as pl
from jax.experimental.pallas import tpu as pltpu
from jax.sharding import PartitionSpec as P

norm_eps = 1e-06
MESH = pl.DeviceIdType.MESH
F32 = jnp.float32
BF16 = jnp.bfloat16


def scaled_norm(row_data, gain_vec):
    values = row_data.astype(F32)
    inverse = lax.rsqrt(jnp.mean(values * values, axis=1, keepdims=True) + norm_eps)
    return (values * inverse * gain_vec.astype(F32)).astype(BF16)


def expert_kernel(
    x_ref, wg_ref, wu_ref, wd_ref, out_ref,
    wgp, wup, wdp, ag, ag4, part, part4, own, rs,
    w_send, w_recv, ag_send, ag_recv, rs_send, rs_recv,
):
    ep = lax.axis_index("ep")
    tp = lax.axis_index("tp")
    count = lax.axis_size("tp")
    right = lax.rem(tp + 2, count)
    left = lax.rem(tp + count - 2, count)
    partner = tp + 1 - 2 * lax.rem(tp, 2)
    width = x_ref.shape[1]
    half = width // 2

    barrier = pltpu.get_barrier_semaphore()
    for other in (left, right, partner):
        pl.semaphore_signal(barrier, inc=1, device_id=(ep, other), device_id_type=MESH)
    pl.semaphore_wait(barrier, 3)

    towards = (right, left)

    def copy(src, dst, send, recv, target):
        return pltpu.make_async_remote_copy(
            src_ref=src, dst_ref=dst, send_sem=send, recv_sem=recv,
            device_id=(ep, target), device_id_type=MESH,
        )

    def cols(h):
        return pl.ds(h * half, half)

    gather = {}
    for direction in (0, 1):
        for step in range(1, 5):
            for h in ((0, 1) if step < 4 else (direction,)):
                index = (step - 1) * 2 + (h if step < 4 else 0)
                src = x_ref.at[:, cols(h)] if step == 1 else ag.at[step - 2, direction, :, cols(h)]
                dst = ag.at[step - 1, direction, :, cols(h)] if step < 4 else ag4.at[:, cols(h)]
                gather[direction, step, h] = copy(
                    src, dst, ag_send.at[direction, index], ag_recv.at[direction, index], towards[direction]
                )
    for h in (0, 1):
        for direction in (0, 1):
            gather[direction, 1, h].start()
    weights = [
        copy(wg_ref, wgp, w_send.at[0], w_recv.at[0], partner),
        copy(wu_ref, wup, w_send.at[1], w_recv.at[1], partner),
        copy(wd_ref, wdp, w_send.at[2], w_recv.at[2], partner),
    ]
    for c in weights:
        c.start()

    def ffn(x):
        total = None
        for gate, up, down in ((wg_ref, wu_ref, wd_ref), (wgp, wup, wdp)):
            g = jnp.dot(x, gate[...], preferred_element_type=F32)
            u = jnp.dot(x, up[...], preferred_element_type=F32)
            hidden = (g / (1.0 + jnp.exp(-g)) * u).astype(BF16)
            term = jnp.dot(hidden, down[...], preferred_element_type=F32)
            total = term if total is None else total + term
        return total

    for c in weights:
        c.wait_recv()
    own[...] = ffn(x_ref[...])

    rows = x_ref.shape[0]
    for step in range(1, 4):
        for h in (0, 1):
            for direction in (0, 1):
                gather[direction, step, h].wait_recv()
                if step < 3 or h == direction:
                    gather[direction, step + 1, h].start()
        x = ag[step - 1].reshape(2 * rows, width)
        part[step - 1] = ffn(x).astype(BF16).reshape(2, rows, width)

    scatter = {}
    for direction in (0, 1):
        for step in range(4):
            for h in ((0, 1) if step > 0 else (direction,)):
                index = 0 if step == 0 else step * 2 - 1 + h
                src = part4.at[:, cols(h)] if step == 0 else part.at[3 - step, 1 - direction, :, cols(h)]
                scatter[direction, step, h] = copy(
                    src, rs.at[step, direction, :, cols(h)],
                    rs_send.at[direction, index], rs_recv.at[direction, index], towards[direction],
                )
    for direction in (0, 1):
        scatter[direction, 1, 1 - direction].start()
    for direction in (0, 1):
        gather[direction, 4, direction].wait_recv()
    part4[...] = ffn(ag4[...]).astype(BF16)
    for direction in (0, 1):
        scatter[direction, 0, direction].start()
    for direction in (0, 1):
        h = direction
        scatter[direction, 0, h].wait_recv()
        part[2, 1 - direction, :, cols(h)] = (
            part[2, 1 - direction, :, cols(h)].astype(F32) + rs[0, direction, :, cols(h)].astype(F32)
        ).astype(BF16)
        scatter[direction, 1, h].start()
    for step in (2, 3):
        for order in (0, 1):
            for direction in (0, 1):
                h = (1 - direction) if order == 0 else direction
                scatter[direction, step - 1, h].wait_recv()
                part[3 - step, 1 - direction, :, cols(h)] = (
                    part[3 - step, 1 - direction, :, cols(h)].astype(F32)
                    + rs[step - 1, direction, :, cols(h)].astype(F32)
                ).astype(BF16)
                scatter[direction, step, h].start()
    for h in (0, 1):
        for direction in (0, 1):
            scatter[direction, 3, h].wait_recv()
    out_ref[...] = (own[...] + rs[3, 0].astype(F32) + rs[3, 1].astype(F32)).astype(BF16)
    for c in list(gather.values()) + weights + list(scatter.values()):
        c.wait_send()


def experts_ring(rows, w_gate, w_up, w_down):
    count, width = rows.shape
    hidden = w_gate.shape[1]
    vmem = pl.BlockSpec(memory_space=pltpu.VMEM)
    dma = pltpu.SemaphoreType.DMA
    return pl.pallas_call(
        expert_kernel,
        out_shape=jax.ShapeDtypeStruct((count, width), BF16),
        in_specs=[vmem] * 4,
        out_specs=vmem,
        scratch_shapes=[
            pltpu.VMEM((width, hidden), BF16),
            pltpu.VMEM((width, hidden), BF16),
            pltpu.VMEM((hidden, width), BF16),
            pltpu.VMEM((3, 2, count, width), BF16),
            pltpu.VMEM((count, width), BF16),
            pltpu.VMEM((3, 2, count, width), BF16),
            pltpu.VMEM((count, width), BF16),
            pltpu.VMEM((count, width), F32),
            pltpu.VMEM((4, 2, count, width), BF16),
            dma((3,)), dma((3,)), dma((2, 7)), dma((2, 7)), dma((2, 7)), dma((2, 7)),
        ],
        compiler_params=pltpu.CompilerParams(
            collective_id=0, has_side_effects=True, vmem_limit_bytes=48 * 1024 * 1024
        ),
        cost_estimate=pl.CostEstimate(flops=80_000_000_000, bytes_accessed=4_000_000, transcendentals=0),
    )(rows, w_gate, w_up, w_down)


def shards(
    mix_tokens, mix_gain, gate_proj, conv_proj, value_proj, conv_taps, out_proj,
    moe_tokens, moe_gain, expert_ids, expert_scores, expert_gate, expert_up, expert_down,
):
    n_ep, n_tp = lax.axis_size("ep"), lax.axis_size("tp")
    ep, tp = lax.axis_index("ep"), lax.axis_index("tp")
    core = lax.rem(tp, 2)
    channels = gate_proj.shape[1]
    width = mix_tokens.shape[1]
    same_core = [list(range(0, n_tp, 2)), list(range(1, n_tp, 2))]
    swap = [(t, t ^ 1) for t in range(n_tp)]
    flat = ("ep", "tp")

    joined = jnp.concatenate([gate_proj.T, conv_proj.T, value_proj.T, out_proj], axis=0)
    piece_rows = joined.shape[0] // n_ep
    piece = lax.dynamic_slice_in_dim(joined, ep * piece_rows, piece_rows, 0)
    column = lax.all_gather(piece, "tp", axis=0, tiled=False, axis_index_groups=same_core)
    weights = lax.all_gather(column, "ep", axis=0, tiled=False)
    taps = lax.all_gather(conv_taps, "tp", axis=0, tiled=False, axis_index_groups=same_core)
    per = channels // piece_rows
    taps = taps.reshape(n_tp // 2, 3, per, piece_rows).transpose(1, 2, 0, 3).reshape(3, -1).astype(F32)

    moe_normed = scaled_norm(moe_tokens, moe_gain)
    experts = n_ep
    row_count, top_count = expert_ids.shape
    capacity = top_count * row_count // experts + max(1, top_count * row_count // (8 * experts))
    flat_ids = expert_ids.reshape(-1)
    onehot = (flat_ids[:, None] == jnp.arange(experts, dtype=jnp.int32)[None, :]).astype(jnp.int32)
    slot_rank = jnp.sum((jnp.cumsum(onehot, axis=0) - onehot) * onehot, axis=1)
    slot_index = flat_ids * capacity + slot_rank
    slot_match = slot_index[:, None] == jnp.arange(experts * capacity, dtype=jnp.int32)[None, :]
    dispatch_map = jnp.any(slot_match.reshape(row_count, top_count, experts * capacity), axis=1).astype(BF16)
    outgoing = lax.dot_general(
        dispatch_map, moe_normed, (((0,), (0,)), ((), ())), preferred_element_type=F32
    ).astype(BF16)
    arrived = lax.all_to_all(
        outgoing.reshape(experts, capacity, width), "ep", split_axis=0, concat_axis=0, tiled=True
    )
    summed = experts_ring(arrived.reshape(-1, width), expert_gate[0], expert_up[0], expert_down[0])
    returned = lax.all_to_all(
        summed.reshape(experts, capacity, width), "ep", split_axis=0, concat_axis=0, tiled=True
    )
    picked = returned.reshape(experts * capacity, width)[slot_index].reshape(row_count, top_count, width)
    route_weight = jax.nn.softmax(expert_scores, axis=1)
    moe_out = jnp.sum(route_weight[:, :, None] * picked.astype(F32), axis=1).astype(BF16)

    normed = scaled_norm(mix_tokens, mix_gain)
    total = n_ep * n_tp
    halo = lax.ppermute(normed[-16:], flat, [(i, i + 1) for i in range(total - 1)])
    both = jnp.concatenate([halo, normed], axis=0)
    theirs = lax.ppermute(both, "tp", swap)
    before = jnp.where(core == 0, halo, theirs[:16])
    rows = jnp.concatenate([before, normed, theirs[16:]], axis=0)
    in_rows = weights[: 3 * n_ep // 4].reshape(-1, width)
    combined = lax.dot_general(
        rows, in_rows, (((1,), (1,)), ((), ())), preferred_element_type=F32
    ).astype(BF16)
    wide = combined.shape[1] // 3
    out_gate = combined[:, :wide]
    signal = (combined[:, wide : 2 * wide].astype(F32) * combined[:, 2 * wide :].astype(F32)).astype(BF16).astype(F32)
    count = normed.shape[0]
    sig_halo, sig_own, sig_their = signal[14:16], signal[16 : 16 + count], signal[16 + count :]
    prev_own = jnp.where(core == 0, sig_halo, sig_their[-2:])
    prev_their = jnp.where(core == 0, sig_own[-2:], sig_halo)

    def carry(prev, sig, gate):
        ext = jnp.concatenate([prev, sig], axis=0)
        conv = jnp.zeros((count, wide), F32)
        for k in range(3):
            conv = conv + ext[k : k + count] * taps[k]
        return (gate.astype(F32) * conv).astype(BF16)

    carried = jnp.concatenate(
        [
            carry(prev_own, sig_own, out_gate[16 : 16 + count]),
            carry(prev_their, sig_their, out_gate[16 + count :]),
        ],
        axis=0,
    )
    out_rows = weights[3 * n_ep // 4 :].reshape(-1, width)
    partial = jnp.dot(carried, out_rows, preferred_element_type=F32)
    other = lax.ppermute(partial[count:].astype(BF16), "tp", swap)
    mix_out = (partial[:count] + other.astype(F32)).astype(BF16)
    return (mix_out, moe_out)


def solution(mesh):
    in_specs = (
        P(("ep", "tp"), None), P(), P(None, "tp"), P(None, "tp"), P(None, "tp"), P(None, "tp"), P("tp", None),
        P(("ep", "tp"), None), P(), P(("ep", "tp"), None), P(("ep", "tp"), None),
        P("ep", None, "tp"), P("ep", None, "tp"), P("ep", "tp", None),
    )
    out_specs = (P(("ep", "tp"), None), P(("ep", "tp"), None))
    return jax.shard_map(shards, mesh=mesh, in_specs=in_specs, out_specs=out_specs, check_vma=False)
```

time: 293 us -> 214 us (0.73)
  waiting for transfers between devices: 190 us -> 11 us
  Pallas kernels: 0 us -> 95.1 us
  matrix products: 34 us -> 3.02 us
  blocking collectives: 23.1 us -> 46.8 us
  local copies, waits for them, and re-layouts: 7.03 us -> 16.7 us
    all_gather x3 -> x1, waiting for transfers between devices: 126 us -> 0.02 us  [shards(): weights = lax.all_gather(column, 'ep', axis=0, tiled=False)]
    pallas_call x0 -> x1, Pallas kernels: none -> 95.1 us  [experts_ring(): pl.pallas_call(expert_kernel, out_shape=jax.ShapeDtypeStruct((count, widt...]
    reduce_scatter x1 -> x0, waiting for transfers between devices: 61.9 us -> none  [shards(): lax.psum_scatter(jnp.dot(hidden, w_down, preferred_element_type=jnp.float...]
    all_gather x0 -> x2, blocking collectives: none -> 46.8 us  [the longest x1 30.9 us: shards(): lax.all_gather(piece, 'tp', axis=0, tiled=False, axis_index_groups=same_c...]
    dot_general x4 -> x2, matrix products: 32.7 us -> 2.64 us  [the longest x1 1.93 us: shards(): lax.dot_general(rows, in_rows, (((1,), (1,)), ((), ())), preferred_elemen...]
    all_to_all x1 -> x0, blocking collectives: 23.1 us -> none  [shards(): lax.all_to_all(outgoing.reshape(experts, capacity, width_model), 'ep', sp...]
    all_to_all x2, waiting for transfers between devices: 0.01 us -> 10.9 us  [the longest x1 6.08 us: shards(): lax.all_to_all(outgoing.reshape(experts, capacity, width), 'ep', split_ax...]
    slice x1 -> x12, local copies, waits for them, and re-layouts: 0.08 us -> 5.51 us  [the longest x2 1.94 us: shards(): in_rows = weights[:3 * n_ep // 4].reshape(-1, width)]
  transfers between devices with their start and end apart: 7 -> 6, of which waited for: 5 -> 2; matrix products, arithmetic and copies ran while one was open for 13% -> 10% of each run, Pallas kernels for 0% -> 45%
where the time goes in v1:
time: 214 us; the launch traced here: 212 us
  Pallas kernels  95.1 us (44%)
  blocking collectives  46.8 us (22%)
  local copies, waits for them, and re-layouts  16.7 us (8%)
  starting transfers between devices  15.6 us (7%)
  between operations  14.4 us (7%)
  waiting for transfers between devices  11 us (5%)
  other arithmetic  9.63 us (5%)
  matrix products  3.02 us (1%)
    pallas_call x1, Pallas kernels, experts_ring(): pl.pallas_call(expert_kernel, out_shape=jax.ShapeDtypeStruct((count, widt...  95.1 us
    all_gather x1, blocking collectives, shards(): lax.all_gather(piece, 'tp', axis=0, tiled=False, axis_index_groups=same_c...  30.9 us
    all_gather x1, blocking collectives, shards(): lax.all_gather(conv_taps, 'tp', axis=0, tiled=False, axis_index_groups=sa...  15.9 us
    all_to_all x1, starting transfers between devices, shards(): lax.all_to_all(outgoing.reshape(experts, capacity, width), 'ep', split_ax...  7.47 us
    all_to_all x1, starting transfers between devices, shards(): lax.all_to_all(summed.reshape(experts, capacity, width), 'ep', split_axis...  6.19 us
    all_to_all x1, waiting for transfers between devices, shards(): lax.all_to_all(outgoing.reshape(experts, capacity, width), 'ep', split_ax...  6.08 us
    all_to_all x1, waiting for transfers between devices, shards(): lax.all_to_all(summed.reshape(experts, capacity, width), 'ep', split_axis...  4.85 us
  transfers between devices with their start and end apart: 6, of which 2 were waited for; matrix products, arithmetic and copies ran while one was open for 10% of the time, Pallas kernels for 45%

profile of v1, /device:TPU:2, one launch (start us, length us, event | category | flops | bytes accessed | tf_op | source)
XLA Modules:
  0.0 212.3 jit_solution(4985058382710666656)
XLA Ops:
  7.3 1.0 fusion.37
  8.3 30.9 %all-gather = bf16[128,2048]{1,0:T(8,128)(2,1)} all-gather(bf16[16,2048]{1,0:T(8,128)(2,1)S(1)} %fusion.37), channel_id=2, replica_groups={{0,2,4,6,8,10,12,14},{1,3,5,7,9,11,13,15},{16,18,20,22,24,26,28,30},{17..., dimensions={0}, use_global_device_ids=true | all-gather | bytes 589824 | tf_op jit(solution)/shard_map/all_gather | solution.py:182
  39.7 1.9 collective-permute-start
  43.2 1.2 reshape.103
  44.4 7.5 %all-to-all-start = ((bf16[16,9,2048]{2,1,0:T(8,128)(2,1)}), bf16[16,9,2048]{2,1,0:T(8,128)(2,1)}, u32[]{:S(2)}, u32[]{:S(2)}) async-start(bf16[16,9,2048]{2,1,0:T(8,128)(2,1)} %reshape.103), calls=%async_computation | async-start | bytes 2097152 | tf_op jit(solution)/shard_map/all_to_all | solution.py:201
  51.9 15.9 %all-gather.3 = bf16[8,3,64]{2,1,0:T(4,128)(2,1)S(1)} all-gather(bf16[1,3,64]{2,1,0:T(4,128)(2,1)S(1)} %bitcast.38), channel_id=4, replica_groups={{0,2,4,6,8,10,12,14},{1,3,5,7,9,11,13,15},{16,18,20,22,24,26,28,30},{17..., dimensions={0}, use_global_device_ids=true | all-gather | bytes 3456 | tf_op jit(solution)/shard_map/all_gather | solution.py:184
  68.5 0.9 pad_maximum_fusion
  69.4 6.1 %all-to-all-done = bf16[16,9,2048]{2,1,0:T(8,128)(2,1)} async-done(((bf16[16,9,2048]{2,1,0:T(8,128)(2,1)}), bf16[16,9,2048]{2,1,0:T(8,128)(2,1)}, u32[]{:S(2)}, u32[]{:S(2)}) %all-to-all-start) | async-done | bytes 589856 | tf_op jit(solution)/shard_map/all_to_all | solution.py:201
  75.5 1.5 reshape.104.x_ref
  77.0 1.2 copy-done.2
  78.2 95.1 %shard_map.149 = bf16[144,2048]{1,0:T(8,128)(2,1)S(1)} custom-call(bf16[144,2048]{1,0:T(8,128)(2,1)S(1)} %reshape.104.x_ref, bf16[2048,256]{1,0:T(8,128)(2,1)S(1)} %bitcast.28, bf16[2048,256]{1,0:T(8,128)(2,1)S(1)} %bitcast.29, bf16[256,2048]{1,0:T(8,128)(2,1)S(1)} %bitcast.30), custom_call_target="tpu_custom_call" | custom-call | flops 80000000000 | bytes 4000000 | tf_op jit(solution)/shard_map/pallas_call | solution.py:142
  173.3 1.2 reshape.105
  174.5 6.2 %all-to-all-start.1 = ((bf16[16,9,2048]{2,1,0:T(8,128)(2,1)}), bf16[16,9,2048]{2,1,0:T(8,128)(2,1)}, u32[]{:S(2)}, u32[]{:S(2)}) async-start(bf16[16,9,2048]{2,1,0:T(8,128)(2,1)} %reshape.105), calls=%async_computation.1 | async-start | bytes 2097152 | tf_op jit(solution)/shard_map/all_to_all | solution.py:205
  180.7 1.1 slice.110
  182.7 1.0 copy-done.4
  183.7 1.9 slice-done
  185.6 1.9 convolution_convert_fusion
  187.9 1.6 slice-done.1
  191.1 4.9 %all-to-all-done.1 = bf16[16,9,2048]{2,1,0:T(8,128)(2,1)} async-done(((bf16[16,9,2048]{2,1,0:T(8,128)(2,1)}), bf16[16,9,2048]{2,1,0:T(8,128)(2,1)}, u32[]{:S(2)}, u32[]{:S(2)}) %all-to-all-start.1) | async-done | bytes 589856 | tf_op jit(solution)/shard_map/all_to_all | solution.py:205
  195.9 1.5 reshape.106
  197.4 0.9 gather_fusion
  198.4 1.6 reshape.107
  200.0 3.5 %multiply_reduce_fusion = bf16[64,2048]{1,0:T(8,128)(2,1)} fusion(f32[64,2,2048]{2,1,0:T(2,128)} %reshape.107, f32[64,2]{1,0:T(8,128)S(1)} %copy.45), kind=kLoop, calls=%fused_computation.16 | loop fusion | flops 393216 | bytes 1311232 | tf_op jit(solution)/shard_map/reduce_sum | solution.py:210
  203.5 1.9 fusion.8
  (73 shorter events, 5.5 us)
Async XLA Ops:
  7.2 32.0 %copy-start.8 = (bf16[2048]{0:T(1024)(128)(2,1)S(1)}, bf16[2048]{0:T(1024)(128)(2,1)}, u32[]{:S(2)}) copy-start(bf16[2048]{0:T(1024)(128)(2,1)} %param.15) | copy-start | bytes 12292
  7.2 32.1 %copy-start.5 = (bf16[128,2048]{1,0:T(8,128)(2,1)S(1)}, bf16[128,2048]{1,0:T(8,128)(2,1)}, u32[]{:S(2)}) copy-start(bf16[128,2048]{1,0:T(8,128)(2,1)} %param.14) | copy-start | bytes 1572868
  7.2 34.4 %copy-start.10 = (s32[64,2]{0,1:T(2,128)S(1)}, s32[64,2]{0,1:T(2,128)}, u32[]{:S(2)}) copy-start(s32[64,2]{0,1:T(2,128)} %param.23) | copy-start | bytes 1540
  7.2 175.5 %all-gather.6.cloned.1.call-start = ((), (), s32[]{:S(2)}) async-start(), calls=%async_computation.2 | async-start | bytes 8912896 | tf_op jit(solution)/shard_map/all_gather | solution.py:183
  7.2 35.3 %copy-start.9 = (bf16[2048]{0:T(1024)(128)(2,1)S(1)}, bf16[2048]{0:T(1024)(128)(2,1)}, u32[]{:S(2)}) copy-start(bf16[2048]{0:T(1024)(128)(2,1)} %param.22) | copy-start | bytes 12292
  7.3 35.4 %copy-start.6 = (bf16[64,2048]{1,0:T(8,128)(2,1)S(1)}, bf16[64,2048]{1,0:T(8,128)(2,1)}, u32[]{:S(2)}) copy-start(bf16[64,2048]{1,0:T(8,128)(2,1)} %param.21) | copy-start | bytes 786436
  39.6 28.9 %copy-start.3 = (bf16[128,2048]{1,0:T(8,128)(2,1)}, bf16[128,2048]{1,0:T(8,128)(2,1)S(1)}, u32[]{:S(2)}) copy-start(bf16[128,2048]{1,0:T(8,128)(2,1)S(1)} %fusion.7) | copy-start | bytes 1572868
  39.7 28.8 %collective-permute-start = (bf16[16,2048]{1,0:T(8,128)(2,1)S(1)}, bf16[16,2048]{1,0:T(8,128)(2,1)S(1)}, u32[]{:S(2)}, u32[]{:S(2)}) collective-permute-start(bf16[16,2048]{1,0:T(8,128)(2,1)S(1)} %slice.108), channel_id=1, source_target_pairs={{0,1},{1,2},{2,3},{3,4},{4,5},{5,6},{6,7},{7,8},{8,9},{9,10},{10,1... | collective-permute-start | bytes 196616 | tf_op jit(solution)/shard_map/ppermute | solution.py:214
  42.8 9.1 %copy-start.11 = (bf16[3,64]{1,0:T(4,128)(2,1)S(1)}, bf16[3,64]{1,0:T(4,128)(2,1)}, u32[]{:S(2)}) copy-start(bf16[3,64]{1,0:T(4,128)(2,1)} %param.19) | copy-start | bytes 1156
  43.2 24.7 %copy-start.7 = (f32[64,2]{0,1:T(2,128)S(1)}, f32[64,2]{0,1:T(2,128)}, u32[]{:S(2)}) copy-start(f32[64,2]{0,1:T(2,128)} %param.24) | copy-start | bytes 1540
  44.4 31.0 %all-to-all-start = ((bf16[16,9,2048]{2,1,0:T(8,128)(2,1)}), bf16[16,9,2048]{2,1,0:T(8,128)(2,1)}, u32[]{:S(2)}, u32[]{:S(2)}) async-start(bf16[16,9,2048]{2,1,0:T(8,128)(2,1)} %reshape.103), calls=%async_computation | async-start | bytes 2097152 | tf_op jit(solution)/shard_map/all_to_all | solution.py:201
  51.9 25.1 %copy-start = (bf16[1,2048,256]{2,1,0:T(8,128)(2,1)S(1)}, bf16[1,2048,256]{2,1,0:T(8,128)(2,1)}, u32[]{:S(2)}) copy-start(bf16[1,2048,256]{2,1,0:T(8,128)(2,1)} %param.25) | copy-start | bytes 3145732
  51.9 25.1 %copy-start.1 = (bf16[1,2048,256]{2,1,0:T(8,128)(2,1)S(1)}, bf16[1,2048,256]{2,1,0:T(8,128)(2,1)}, u32[]{:S(2)}) copy-start(bf16[1,2048,256]{2,1,0:T(8,128)(2,1)} %param.26) | copy-start | bytes 3145732
  69.4 111.3 %collective-permute-start.1 = (bf16[144,2048]{1,0:T(8,128)(2,1)}, bf16[144,2048]{1,0:T(8,128)(2,1)}, u32[]{:S(2)}, u32[]{:S(2)}) collective-permute-start(bf16[144,2048]{1,0:T(8,128)(2,1)} %pad_maximum_fusion), channel_id=1, source_target_pairs={{0,1},{1,0},{2,3},{3,2},{4,5},{5,4},{6,7},{7,6},{8,9},{9,8},{10,11... | collective-permute-start | bytes 1769480 | tf_op jit(solution)/shard_map/ppermute | solution.py:216
  77.0 1.2 copy-start.2
  174.5 21.4 %all-to-all-start.1 = ((bf16[16,9,2048]{2,1,0:T(8,128)(2,1)}), bf16[16,9,2048]{2,1,0:T(8,128)(2,1)}, u32[]{:S(2)}, u32[]{:S(2)}) async-start(bf16[16,9,2048]{2,1,0:T(8,128)(2,1)} %reshape.105), calls=%async_computation.1 | async-start | bytes 2097152 | tf_op jit(solution)/shard_map/all_to_all | solution.py:205
  182.6 1.0 copy-start.4
  182.7 2.9 %slice-start = ((bf16[128,16,2048]{2,1,0:T(8,128)(2,1)}), bf16[96,16,2048]{2,1,0:T(8,128)(2,1)S(1)}, s32[]{:S(2)}) async-start(bf16[128,16,2048]{2,1,0:T(8,128)(2,1)} %all-gather.6.cloned.1.call-done), calls=%async_computation.3 | async-start | bytes 12582912 | tf_op jit(solution)/shard_map/slice | solution.py:219
  187.9 1.6 slice-start.1
  191.1 12.4 %collective-permute-start.2 = (bf16[128,2048]{1,0:T(8,128)(2,1)}, bf16[128,2048]{1,0:T(8,128)(2,1)}, u32[]{:S(2)}, u32[]{:S(2)}) collective-permute-start(bf16[128,2048]{1,0:T(8,128)(2,1)} %slice.176), channel_id=1, source_target_pairs={{0,1},{1,0},{2,3},{3,2},{4,5},{5,4},{6,7},{7,6},{8,9},{9,8},{10,11... | collective-permute-start | bytes 1572872 | tf_op jit(solution)/shard_map/ppermute | solution.py:247
Sparse Core Ops, SparseCore 0:
  39.3 83.2 all-gather.5
